TPU v7x, 32 devices: a whole 2x2x4 slice. The times are simulated.
32 devices in a mesh: sp: 16 (over z, y, x), tp: 2 (over core).
Axes of the slice: x: 2, y: 2, z: 4, core: 2. Of those that a mesh axis runs over, the one named last changes fastest.
Arguments:
- queries: bfloat16 [4096, 8, 128], P('sp', 'tp'), may hold values from -6 to 6
- keys: bfloat16 [4096, 2, 128], P('sp'), may hold values from -6 to 6
- values: bfloat16 [4096, 2, 128], P('sp'), may hold values from -6 to 6
- documents: int32 [4096], P('sp'), may hold values from 0 to 3, never falling along the last dimension, each value on 1 to 2304 neighbouring positions
- query_gain: float32 [128], replicated, may hold values from 0.25 to 4
- key_gain: float32 [128], replicated, may hold values from 0.25 to 4
- out_weight: bfloat16 [1024, 2048], P('tp'), may hold values from -0.1875 to 0.1875
- residual: bfloat16 [4096, 2048], P('sp'), may hold values from -6 to 6
- norm_gain: float32 [2048], replicated, may hold values from 0.1 to 1.9
- up_weight: bfloat16 [2048, 6144], P('sp', 'tp'), may hold values from -0.125 to 0.125
- down_weight: bfloat16 [2048, 6144], P('sp', 'tp'), may hold values from -0.078125 to 0.078125
Outputs:
- layer_out: bfloat16 [4096, 2048], P(('sp', 'tp'))
Inputs may be any that keep to these rules, and one draw needn't show every extreme that they name: `documents`: document numbers never fall along the sequence; one document covers exactly (9) * 256 positions.
All inputs are finite; a program needn't handle non-finite values.
Results may differ from a plain program's by a relative error of at most 0.017.
Values may be sent and summed in bfloat16 or wider, within the bound.
A program may use at most 128 MiB of HBM per device.

v0:
```python
import functools

import jax
import jax.numpy as jnp
from jax import lax
from jax.experimental import pallas as pl
from jax.experimental.pallas import tpu as pltpu
from jax.sharding import PartitionSpec as P

QUERY_HEADS = 8
GRID = 64


EPS = 1e-06
THETA = 10000.0


def head_norm(block, gain):
    return block * lax.rsqrt(jnp.mean(block * block, axis=-1, keepdims=True) + EPS) * gain


def rotate(block, positions):
    head_width = block.shape[-1]
    pair_count = head_width // 4
    inverse = THETA ** (-jnp.arange(pair_count, dtype=jnp.float32) / pair_count)
    grid_row = (positions // GRID).astype(jnp.float32)[:, None] * inverse
    grid_col = (positions % GRID).astype(jnp.float32)[:, None] * inverse
    angles = jnp.concatenate([grid_row, grid_row, grid_col, grid_col], axis=-1)
    cosine = jnp.cos(angles)[:, None, :]
    sine_table = jnp.sin(angles)[:, None, :]
    turned = jnp.concatenate(
        [
            -block[..., pair_count : 2 * pair_count],
            block[..., 0:pair_count],
            -block[..., 3 * pair_count :],
            block[..., 2 * pair_count : 3 * pair_count],
        ],
        axis=-1,
    )
    return block * cosine + turned * sine_table


def channel_norm(rows_in, gain):
    widened = rows_in.astype(jnp.float32)
    return (
        widened * lax.rsqrt(jnp.mean(widened * widened, axis=-1, keepdims=True) + EPS) * gain
    ).astype(jnp.bfloat16)


def body(
    queries,
    keys,
    values,
    documents,
    query_gain,
    key_gain,
    out_weight,
    residual,
    norm_gain,
    up_weight,
    down_weight,
):
    tok_dev = queries.shape[0]
    heads_here = queries.shape[1]
    head_width = queries.shape[2]
    query_group_count = QUERY_HEADS // keys.shape[1]
    kv_index = lax.axis_index("tp") * heads_here // query_group_count
    positions = lax.axis_index("sp") * tok_dev + jnp.arange(tok_dev, dtype=jnp.int32)
    own_keys = lax.dynamic_index_in_dim(keys, kv_index, 1, keepdims=True)
    own_values = lax.dynamic_index_in_dim(values, kv_index, 1, keepdims=False)
    key_rot = rotate(head_norm(own_keys.astype(jnp.float32), key_gain), positions)[:, 0, :].astype(
        jnp.bfloat16
    )
    rotated_query = rotate(head_norm(queries.astype(jnp.float32), query_gain), positions).astype(
        jnp.bfloat16
    )
    scale = head_width ** (-0.5)
    first_doc = documents[0]
    last_doc = documents[tok_dev - 1]
    start_state = (
        jnp.full((tok_dev, heads_here), -1e30, jnp.float32),
        jnp.zeros((tok_dev, heads_here), jnp.float32),
        jnp.zeros((tok_dev, heads_here, head_width), jnp.float32),
    )
    piece_keys = lax.all_gather(key_rot, "sp", axis=0, tiled=True)
    piece_values = lax.all_gather(own_values, "sp", axis=0, tiled=True)
    piece_docs = lax.all_gather(documents, "sp", axis=0, tiled=True)

    def update(state):
        peak, denom, summed = state
        scores = (
            jnp.einsum("qhd,kd->qhk", rotated_query, piece_keys, preferred_element_type=jnp.float32)
            * scale
        )
        allowed = (documents[:, None] == piece_docs[None, :])[:, None, :]
        scores = jnp.where(allowed, scores, -1e30)
        new_peak = jnp.maximum(peak, jnp.max(scores, axis=-1))
        probs = jnp.where(allowed, jnp.exp(scores - new_peak[..., None]), 0.0)
        denom = jnp.sum(probs, axis=-1)
        summed = jnp.einsum(
            "qhk,kd->qhd",
            probs.astype(jnp.bfloat16),
            piece_values,
            preferred_element_type=jnp.float32,
        )
        return (new_peak, denom, summed)

    touches = jnp.logical_and(
        piece_docs[0] <= last_doc, piece_docs[piece_docs.shape[0] - 1] >= first_doc
    )
    peak, denom, summed = lax.cond(touches, update, lambda state: state, start_state)
    attn = (
        (summed / denom[..., None]).reshape(tok_dev, heads_here * head_width).astype(jnp.bfloat16)
    )
    share = tok_dev // lax.axis_size("tp")
    branch = lax.psum(
        jnp.dot(attn, out_weight, preferred_element_type=jnp.float32).astype(jnp.bfloat16), "tp"
    ).astype(jnp.float32)
    whole_rows = (residual.astype(jnp.float32) + branch).astype(jnp.bfloat16)
    normed = channel_norm(whole_rows, norm_gain)
    mid = lax.dynamic_slice_in_dim(whole_rows, lax.axis_index("tp") * share, share, 0)
    raised = jnp.dot(
        normed,
        lax.all_gather(up_weight, "sp", axis=0, tiled=True),
        preferred_element_type=jnp.float32,
    )
    hidden = jnp.square(jax.nn.relu(raised)).astype(jnp.bfloat16)
    terms = lax.dot_general(
        hidden,
        lax.all_gather(down_weight, "sp", axis=0, tiled=True),
        (((1,), (1,)), ((), ())),
        preferred_element_type=jnp.float32,
    )
    mixer = lax.psum_scatter(
        terms.astype(jnp.bfloat16), "tp", scatter_dimension=0, tiled=True
    ).astype(jnp.float32)
    return (mid.astype(jnp.float32) + mixer).astype(jnp.bfloat16)


MESH = pl.DeviceIdType.MESH
NT = (((1,), (1,)), ((), ()))
F32 = jnp.float32
BF16 = jnp.bfloat16


def layer_kernel(
    q_ref, kv_ref, drow_ref, dcol_ref, ow_ref, res_ref, gain_ref, up_ref, down_ref, out_ref,
    kv_all, doc_all, attn, wup, wdown, part, part_in, mid, norm_all, hidden, outs, outs_in, sums,
    final_in, kv_s, kv_r, dc_s, dc_r, w_s, w_r, loc_s, p_s, p_r, n_s, n_r, o_s, o_r, f_s, f_r,
):
    heads, rows, width = q_ref.shape
    half = rows // 2
    depth, cols = wup.shape[1], wup.shape[2]
    model = ow_ref.shape[1]
    sp, core = lax.axis_index("sp"), lax.axis_index("tp")
    n_z = lax.axis_size("sp") // 4
    x, y, z = sp % 2, (sp // 2) % 2, sp // 4

    def at(dx, dy, r):
        return ((z + r) % n_z * 2 + (y + dy) % 2) * 2 + (x + dx) % 2

    def mate(rc):
        return (((z // 2) * 2 + (z + rc // 2) % 2) * 2 + y) * 2 + (x + rc) % 2

    def rank(spi):
        return (spi // 4) % 2 * 2 + spi % 2

    sent = []

    def send(src, dst, ss, rs, spi, tpi):
        c = pltpu.make_async_remote_copy(
            src_ref=src, dst_ref=dst, send_sem=ss, recv_sem=rs,
            device_id=(spi, tpi), device_id_type=MESH,
        )
        c.start()
        sent.append(c)

    def arrive(dst, ss, rs):
        pltpu.make_async_remote_copy(
            src_ref=dst, dst_ref=dst, send_sem=ss, recv_sem=rs,
            device_id=(sp, 1 - core), device_id_type=MESH,
        ).wait_recv()

    barrier = pltpu.get_barrier_semaphore()
    peers = [(at(dx, 0, k), core) for dx in (0, 1) for k in range(n_z) if dx or k]
    peers += [(at(0, 1, 0), core), (sp, 1 - core)]
    for p in peers:
        pl.semaphore_signal(barrier, inc=1, device_id=p, device_id_type=MESH)
    pl.semaphore_wait(barrier, len(peers))

    def slot(dx, dy, r):
        return (dx * 2 + dy) * n_z + r

    def send_kv(src_slot, dst_slot, spi):
        src = kv_ref if src_slot is None else kv_all.at[src_slot]
        dsrc = drow_ref if src_slot is None else doc_all.at[src_slot]
        i = dst_slot
        send(src, kv_all.at[dst_slot], kv_s.at[i], kv_r.at[i], spi, core)
        send(dsrc, doc_all.at[dst_slot], dc_s.at[i], dc_r.at[i], spi, core)

    def wait_kv(i):
        arrive(kv_all.at[i], kv_s.at[i], kv_r.at[i])
        arrive(doc_all.at[i], dc_s.at[i], dc_r.at[i])

    weights = ((up_ref, wup), (down_ref, wdown))

    def send_weight(w, dx, k):
        src, dst = weights[w]
        target = at(dx, 0, k)
        block = src.at[:, pl.ds(pl.multiple_of(rank(target) * cols, 128), cols)]
        i = dx * n_z + (n_z - k) % n_z
        if dx or k:
            send(block, dst.at[sp], w_s.at[w, i], w_r.at[w, i], target, core)

    def forward_weight(w, i):
        dst = weights[w][1]
        owner = at(i // n_z, 0, i % n_z)
        if i:
            arrive(dst.at[owner], w_s.at[w, i], w_r.at[w, i])
        j = 2 * n_z + i
        send(dst.at[owner], dst.at[owner], w_s.at[w, j], w_r.at[w, j], at(0, 1, 0), core)

    def last_weight(w):
        dst = weights[w][1]
        for i in range(2 * n_z):
            owner = at(i // n_z, 1, i % n_z)
            arrive(dst.at[owner], w_s.at[w, 2 * n_z + i], w_r.at[w, 2 * n_z + i])

    for k in range(1, n_z):
        send_kv(None, slot(0, 0, n_z - k), at(0, 0, k))
    send_kv(None, slot(1, 0, 0), at(1, 0, 0))
    send_kv(None, slot(0, 1, 0), at(0, 1, 0))
    own = []
    for w in (0, 1):
        src, dst = weights[w]
        block = src.at[:, pl.ds(pl.multiple_of(rank(sp) * cols, 128), cols)]
        own.append(pltpu.make_async_copy(block, dst.at[sp], loc_s.at[w]))
    own.append(pltpu.make_async_copy(kv_ref, kv_all.at[0], loc_s.at[2]))
    own.append(pltpu.make_async_copy(drow_ref, doc_all.at[0], loc_s.at[3]))
    for c in own:
        c.start()
    near = sorted(range(1, n_z), key=lambda r: min(r, n_z - r))
    for k in near:
        send_weight(0, 0, k)
    for r in near:
        wait_kv(slot(0, 0, r))
        send_kv(slot(0, 0, r), slot(1, 0, r), at(1, 0, 0))
        send_kv(slot(0, 0, r), slot(0, 1, r), at(0, 1, 0))
    for r in [0] + near:
        wait_kv(slot(1, 0, r))
        if r < n_z // 2:
            send_kv(slot(1, 0, r), slot(1, 1, r), at(0, 1, 0))
        wait_kv(slot(0, 1, r))
        if r >= n_z // 2:
            send_kv(slot(0, 1, r), slot(1, 1, r), at(1, 0, 0))
    for c in own:
        c.wait()
    for k in [0] + near:
        send_weight(0, 1, k)
    for k in near:
        send_weight(1, 0, k)
    for k in [0] + near:
        send_weight(1, 1, k)
    order = [dx * n_z + r for dx in (0, 1) for r in [0] + near]
    forward_weight(0, order[0])
    for r in range(n_z):
        wait_kv(slot(1, 1, r))

    scale = width ** (-0.5)
    n_slots = kv_all.shape[0]
    todo = order[1:]
    for h in range(heads):

        def step(i, state):
            peak, denom, acc = state
            scores = lax.dot_general(q_ref[h], kv_all[i, 0], NT, preferred_element_type=F32) * scale
            allowed = dcol_ref[...] == doc_all[i]
            scores = jnp.where(allowed, scores, -1e30)
            new_peak = jnp.maximum(peak, jnp.max(scores, axis=-1, keepdims=True))
            probs = jnp.where(allowed, jnp.exp(scores - new_peak), 0.0)
            decay = jnp.exp(peak - new_peak)
            denom = denom * decay + jnp.sum(probs, axis=-1, keepdims=True)
            acc = acc * decay + jnp.dot(
                probs.astype(BF16), kv_all[i, 1], preferred_element_type=F32
            )
            return new_peak, denom, acc

        state = (
            jnp.full((rows, 1), -1e30, F32),
            jnp.zeros((rows, 1), F32),
            jnp.zeros((rows, width), F32),
        )
        peak, denom, acc = lax.fori_loop(0, n_slots, step, state)
        attn[:, h * width : (h + 1) * width] = (acc / denom).astype(BF16)
        if h >= heads // 2:
            for i in todo[:2]:
                forward_weight(0, i)
            todo = todo[2:]

    tile = 256

    @pl.loop(0, model // tile)
    def _(t):
        lanes = pl.ds(pl.multiple_of(t * tile, tile), tile)
        p = jnp.dot(attn[...], ow_ref[:, lanes], preferred_element_type=F32).astype(BF16)
        part[0, :, lanes] = p[:half]
        part[1, :, lanes] = p[half:]

    send(part.at[1 - core], part_in, p_s, p_r, sp, 1 - core)
    arrive(part_in, p_s, p_r)
    start = pl.ds(pl.multiple_of(core * half, half), half)
    group = 32

    @pl.loop(0, half // group)
    def _(t):
        rws = pl.ds(pl.multiple_of(t * group, group), group)
        branch = part[core, rws].astype(F32) + part_in[rws].astype(F32)
        rres = pl.ds(pl.multiple_of(core * half + t * group, group), group)
        m = (res_ref[rres].astype(F32) + branch).astype(BF16)
        mid[rws] = m
        wide = m.astype(F32)
        inv = lax.rsqrt(jnp.mean(wide * wide, axis=-1, keepdims=True) + EPS)
        norm_all[0, 0, rws] = (wide * inv * gain_ref[...]).astype(BF16)

    for rc in (3, 1, 2):
        send(norm_all.at[0, 0], norm_all.at[rc, 0], n_s.at[rc], n_r.at[rc], mate(rc), core)
    send(norm_all.at[0, 0], norm_all.at[0, 1], n_s.at[4], n_r.at[4], sp, 1 - core)
    for i in todo:
        forward_weight(0, i)
    for i in order[:1] + order[1:5]:
        forward_weight(1, i)
    for rc in (1, 2, 3):
        arrive(norm_all.at[rc, 0], n_s.at[rc], n_r.at[rc])
        j = 4 + rc
        send(norm_all.at[rc, 0], norm_all.at[rc, 1], n_s.at[j], n_r.at[j], sp, 1 - core)
    for i in order[5:]:
        forward_weight(1, i)
    last_weight(0)
    for rc in range(4):
        arrive(norm_all.at[rc, 1], n_s.at[4 + rc], n_r.at[4 + rc])

    @pl.loop(0, 4 * (cols // tile))
    def _(t):
        rc, c = t // (cols // tile), t % (cols // tile)
        lanes = pl.ds(pl.multiple_of(c * tile, tile), tile)
        tokens = norm_all[rc].reshape(rows, model)
        w = wup[:, :, lanes].reshape(model, tile)
        raised = jnp.dot(tokens, w, preferred_element_type=F32)
        hidden[rc, :, lanes] = jnp.square(jnp.maximum(raised, 0.0)).astype(BF16)

    last_weight(1)
    blocks = tile // depth

    for rc in (3, 1, 2, 0):

        @pl.loop(0, model // tile)
        def _(t):
            lanes = pl.ds(pl.multiple_of(t * tile, tile), tile)
            w = wdown[pl.ds(t * blocks, blocks)].reshape(tile, cols)
            o = lax.dot_general(hidden[rc], w, NT, preferred_element_type=F32).astype(BF16)
            outs[rc, 0, :, lanes] = o[:half]
            outs[rc, 1, :, lanes] = o[half:]

        send(outs.at[rc, 1], outs_in.at[rc], o_s.at[rc], o_r.at[rc], sp, 1 - core)

    for rc in (3, 1, 2, 0):
        arrive(outs_in.at[rc], o_s.at[rc], o_r.at[rc])
        if rc:

            @pl.loop(0, half // group)
            def _(t):
                rws = pl.ds(pl.multiple_of(t * group, group), group)
                sums[rc - 1, rws] = (
                    outs[rc, 0, rws].astype(F32) + outs_in[rc, rws].astype(F32)
                ).astype(BF16)

            send(sums.at[rc - 1], final_in.at[rc - 1], f_s.at[rc], f_r.at[rc], mate(rc), core)
    for rc in (1, 2, 3):
        arrive(final_in.at[rc - 1], f_s.at[rc], f_r.at[rc])

    @pl.loop(0, half // group)
    def _(t):
        rws = pl.ds(pl.multiple_of(t * group, group), group)
        total = outs[0, 0, rws].astype(F32) + outs_in[0, rws].astype(F32)
        for rc in range(3):
            total += final_in[rc, rws].astype(F32)
        out_ref[rws] = (mid[rws].astype(F32) + total).astype(BF16)

    for c in sent:
        c.wait_send()


def fused_body(
    queries, keys, values, documents, query_gain, key_gain, out_weight, residual, norm_gain,
    up_weight, down_weight,
):
    rows, heads, width = queries.shape
    n_sp = lax.axis_size("sp")
    model = residual.shape[1]
    depth, cols = up_weight.shape[0], up_weight.shape[1] // 4
    half = rows // 2
    kv_index = lax.axis_index("tp") * heads // (QUERY_HEADS // keys.shape[1])
    positions = lax.axis_index("sp") * rows + jnp.arange(rows, dtype=jnp.int32)
    own_keys = lax.dynamic_index_in_dim(keys, kv_index, 1, keepdims=True)
    own_values = lax.dynamic_index_in_dim(values, kv_index, 1, keepdims=False)
    key_rot = rotate(head_norm(own_keys.astype(F32), key_gain), positions)[:, 0, :].astype(BF16)
    query_rot = rotate(head_norm(queries.astype(F32), query_gain), positions).astype(BF16)
    vm = pl.BlockSpec(memory_space=pltpu.VMEM)
    dma = pltpu.SemaphoreType.DMA
    token = (half, model)
    return pl.pallas_call(
        layer_kernel,
        out_shape=jax.ShapeDtypeStruct(token, BF16),
        in_specs=[vm] * 9,
        out_specs=vm,
        scratch_shapes=[
            pltpu.VMEM((n_sp, 2, rows, width), BF16),
            pltpu.VMEM((n_sp, 1, rows), jnp.int32),
            pltpu.VMEM((rows, heads * width), BF16),
            pltpu.VMEM((n_sp, depth, cols), BF16),
            pltpu.VMEM((n_sp, depth, cols), BF16),
            pltpu.VMEM((2,) + token, BF16),
            pltpu.VMEM(token, BF16),
            pltpu.VMEM(token, BF16),
            pltpu.VMEM((4, 2) + token, BF16),
            pltpu.VMEM((4, rows, cols), BF16),
            pltpu.VMEM((4, 2) + token, BF16),
            pltpu.VMEM((4,) + token, BF16),
            pltpu.VMEM((3,) + token, BF16),
            pltpu.VMEM((3,) + token, BF16),
            dma((n_sp,)), dma((n_sp,)), dma((n_sp,)), dma((n_sp,)),
            dma((2, n_sp)), dma((2, n_sp)), dma((4,)),
            dma, dma, dma((8,)), dma((8,)), dma((4,)), dma((4,)), dma((4,)), dma((4,)),
        ],
        compiler_params=pltpu.CompilerParams(
            collective_id=0, has_side_effects=True, vmem_limit_bytes=60 * 1024 * 1024
        ),
    )(
        query_rot.transpose(1, 0, 2),
        jnp.stack([key_rot, own_values]),
        documents[None, :],
        documents[:, None],
        out_weight,
        residual,
        norm_gain[None, :],
        up_weight,
        down_weight,
    )


def solution(mesh):
    in_specs = (
        P("sp", "tp", None),
        P("sp", None, None),
        P("sp", None, None),
        P("sp"),
        P(),
        P(),
        P("tp", None),
        P("sp", None),
        P(),
        P("sp", "tp"),
        P("sp", "tp"),
    )
    out_specs = P(("sp", "tp"), None)
    fused = mesh.shape["tp"] == 2 and mesh.shape["sp"] == 16
    return jax.shard_map(fused_body if fused else body, mesh=mesh, in_specs=in_specs, out_specs=out_specs, check_vma=False)
```

profile of v0, /device:TPU:0, one launch (start us, length us, event | category | flops | bytes accessed | tf_op | source)
XLA Modules:
  0.0 180.5 jit_solution(4227937807016906134)
XLA Ops:
  0.0 0.0 copy-start.2
  0.0 1.3 constant_dynamic-slice_fusion
  1.3 0.0 copy-start
  1.3 0.0 copy-start.3
  1.3 0.1 fusion.5
  1.4 0.8 fusion.6
  2.2 0.2 slice_negate_fusion.3
  2.4 0.1 fusion.10
  2.5 0.0 copy-done.2
  2.5 0.6 fusion.9
  3.2 0.7 pad_maximum_fusion.2.kv_ref
  3.9 0.6 fusion.13
  4.4 0.0 copy-done
  4.4 0.2 fusion
  4.7 0.0 copy-done.3
  4.7 0.2 fusion.1
  4.9 0.5 slice_negate_fusion.1
  5.4 0.0 copy-start.1
  5.4 1.3 fusion.4.q_ref
  6.7 0.0 copy-done.1
  6.7 0.8 copy.17.dcol_ref
  7.5 171.1 %shard_map.109 = bf16[128,2048]{1,0:T(8,128)(2,1)} custom-call(bf16[4,256,128]{2,1,0:T(8,128)(2,1)} %fusion.4.q_ref, bf16[2,256,128]{2,1,0:T(8,128)(2,1)} %pad_maximum_fusion.2.kv_ref, s32[1,256]{1,0:T(1,128)} %bitcast.16, s32[256,1]{1,0:T(8,128)} %copy.17.dcol_ref, bf16[512,2048]{1,0:T(8,128)(2,1)} %ow_ref.1, bf16[256,2048]{1,0:T(8,128)(2,1)} %res_ref.1, ...), custom_call_target="tpu_custom_call" | custom-call | tf_op jit(solution)/shard_map/pallas_call | solution.py:411
  178.6 1.9 %copy.31 = bf16[128,2048]{1,0:T(8,128)(2,1)} copy(bf16[128,2048]{1,0:T(8,128)(2,1)} %shard_map.109) | data formatting | bytes 1048576
  (5 shorter events, 0.0 us)
Async XLA Ops:
  0.0 2.5 %copy-start.2 = (f32[128]{0:T(128)S(1)}, f32[128]{0:T(128)}, u32[]{:S(2)}) copy-start(f32[128]{0:T(128)} %param.16) | copy-start | bytes 1540
  1.3 3.2 %copy-start = (bf16[256,4,128]{2,1,0:T(4,128)(2,1)S(1)}, bf16[256,4,128]{2,1,0:T(4,128)(2,1)}, u32[]{:S(2)}) copy-start(bf16[256,4,128]{2,1,0:T(4,128)(2,1)} %param.11) | copy-start | bytes 786436
  1.3 3.4 %copy-start.3 = (f32[128]{0:T(128)S(1)}, f32[128]{0:T(128)}, u32[]{:S(2)}) copy-start(f32[128]{0:T(128)} %param.15) | copy-start | bytes 1540
  5.4 1.3 copy-start.1
where the time goes:
time: 181 us; the launch traced here: 180 us
  Pallas kernels  171 us (94%)
  other arithmetic  5.26 us (3%)
  local copies, waits for them, and re-layouts  3.97 us (2%)
    pallas_call x1, Pallas kernels, fused_body(): pl.pallas_call(layer_kernel, out_shape=jax.ShapeDtypeStruct(token, BF16),...  171 us

commit v1 on v0

v1 whole, which is shorter than its diff:
```python
import functools

import jax
import jax.numpy as jnp
import numpy as np
from jax import lax
from jax.experimental import pallas as pl
from jax.experimental.pallas import tpu as pltpu
from jax.sharding import PartitionSpec as P

QUERY_HEADS = 8
GRID = 64


EPS = 1e-06
THETA = 10000.0


def head_norm(block, gain):
    return block * lax.rsqrt(jnp.mean(block * block, axis=-1, keepdims=True) + EPS) * gain


def rotate(block, positions):
    head_width = block.shape[-1]
    pair_count = head_width // 4
    inverse = THETA ** (-jnp.arange(pair_count, dtype=jnp.float32) / pair_count)
    grid_row = (positions // GRID).astype(jnp.float32)[:, None] * inverse
    grid_col = (positions % GRID).astype(jnp.float32)[:, None] * inverse
    angles = jnp.concatenate([grid_row, grid_row, grid_col, grid_col], axis=-1)
    cosine = jnp.cos(angles)[:, None, :]
    sine_table = jnp.sin(angles)[:, None, :]
    turned = jnp.concatenate(
        [
            -block[..., pair_count : 2 * pair_count],
            block[..., 0:pair_count],
            -block[..., 3 * pair_count :],
            block[..., 2 * pair_count : 3 * pair_count],
        ],
        axis=-1,
    )
    return block * cosine + turned * sine_table


def channel_norm(rows_in, gain):
    widened = rows_in.astype(jnp.float32)
    return (
        widened * lax.rsqrt(jnp.mean(widened * widened, axis=-1, keepdims=True) + EPS) * gain
    ).astype(jnp.bfloat16)


def body(
    queries,
    keys,
    values,
    documents,
    query_gain,
    key_gain,
    out_weight,
    residual,
    norm_gain,
    up_weight,
    down_weight,
):
    tok_dev = queries.shape[0]
    heads_here = queries.shape[1]
    head_width = queries.shape[2]
    query_group_count = QUERY_HEADS // keys.shape[1]
    kv_index = lax.axis_index("tp") * heads_here // query_group_count
    positions = lax.axis_index("sp") * tok_dev + jnp.arange(tok_dev, dtype=jnp.int32)
    own_keys = lax.dynamic_index_in_dim(keys, kv_index, 1, keepdims=True)
    own_values = lax.dynamic_index_in_dim(values, kv_index, 1, keepdims=False)
    key_rot = rotate(head_norm(own_keys.astype(jnp.float32), key_gain), positions)[:, 0, :].astype(
        jnp.bfloat16
    )
    rotated_query = rotate(head_norm(queries.astype(jnp.float32), query_gain), positions).astype(
        jnp.bfloat16
    )
    scale = head_width ** (-0.5)
    first_doc = documents[0]
    last_doc = documents[tok_dev - 1]
    start_state = (
        jnp.full((tok_dev, heads_here), -1e30, jnp.float32),
        jnp.zeros((tok_dev, heads_here), jnp.float32),
        jnp.zeros((tok_dev, heads_here, head_width), jnp.float32),
    )
    piece_keys = lax.all_gather(key_rot, "sp", axis=0, tiled=True)
    piece_values = lax.all_gather(own_values, "sp", axis=0, tiled=True)
    piece_docs = lax.all_gather(documents, "sp", axis=0, tiled=True)

    def update(state):
        peak, denom, summed = state
        scores = (
            jnp.einsum("qhd,kd->qhk", rotated_query, piece_keys, preferred_element_type=jnp.float32)
            * scale
        )
        allowed = (documents[:, None] == piece_docs[None, :])[:, None, :]
        scores = jnp.where(allowed, scores, -1e30)
        new_peak = jnp.maximum(peak, jnp.max(scores, axis=-1))
        probs = jnp.where(allowed, jnp.exp(scores - new_peak[..., None]), 0.0)
        denom = jnp.sum(probs, axis=-1)
        summed = jnp.einsum(
            "qhk,kd->qhd",
            probs.astype(jnp.bfloat16),
            piece_values,
            preferred_element_type=jnp.float32,
        )
        return (new_peak, denom, summed)

    touches = jnp.logical_and(
        piece_docs[0] <= last_doc, piece_docs[piece_docs.shape[0] - 1] >= first_doc
    )
    peak, denom, summed = lax.cond(touches, update, lambda state: state, start_state)
    attn = (
        (summed / denom[..., None]).reshape(tok_dev, heads_here * head_width).astype(jnp.bfloat16)
    )
    share = tok_dev // lax.axis_size("tp")
    branch = lax.psum(
        jnp.dot(attn, out_weight, preferred_element_type=jnp.float32).astype(jnp.bfloat16), "tp"
    ).astype(jnp.float32)
    whole_rows = (residual.astype(jnp.float32) + branch).astype(jnp.bfloat16)
    normed = channel_norm(whole_rows, norm_gain)
    mid = lax.dynamic_slice_in_dim(whole_rows, lax.axis_index("tp") * share, share, 0)
    raised = jnp.dot(
        normed,
        lax.all_gather(up_weight, "sp", axis=0, tiled=True),
        preferred_element_type=jnp.float32,
    )
    hidden = jnp.square(jax.nn.relu(raised)).astype(jnp.bfloat16)
    terms = lax.dot_general(
        hidden,
        lax.all_gather(down_weight, "sp", axis=0, tiled=True),
        (((1,), (1,)), ((), ())),
        preferred_element_type=jnp.float32,
    )
    mixer = lax.psum_scatter(
        terms.astype(jnp.bfloat16), "tp", scatter_dimension=0, tiled=True
    ).astype(jnp.float32)
    return (mid.astype(jnp.float32) + mixer).astype(jnp.bfloat16)


MESH = pl.DeviceIdType.MESH
NT = (((1,), (1,)), ((), ()))
F32 = jnp.float32
BF16 = jnp.bfloat16


NEG = -1e30


def rope_tables(n_rows, width):
    quarter = width // 4
    steps = np.arange(quarter, dtype=np.float32) / np.float32(quarter)
    inverse = (np.float32(THETA) ** (-steps)).astype(np.float32)
    tables = []
    for f in (np.cos, np.sin):
        row, col = np.zeros((n_rows, width), np.float32), np.zeros((GRID, width), np.float32)
        for table, at in ((row, 0), (col, 2 * quarter)):
            angle = np.arange(table.shape[0], dtype=np.float32)[:, None] * inverse
            value = f(angle.astype(np.float64))
            table[:, at : at + quarter] = -value if f is np.sin else value
            table[:, at + quarter : at + 2 * quarter] = value
        tables += [row, col]
    return tables


def layer_kernel(
    q_hbm, k_hbm, v_hbm, doc_hbm, qg_hbm, kg_hbm, ow_hbm, res_hbm, ng_hbm, up_hbm, down_hbm,
    cr_hbm, cc_hbm, sr_hbm, sc_hbm, out_ref,
    q_raw, k_raw, v_raw, doc_v, qg, kg, ow, res, ng, cr, cc, sr, sc,
    q_rot, kv_all, dcol, bias, peak_s, den_s, acc_s, attn, wup, wdown, part, part_in, own_part,
    mid, tok, racc, hidden, outs, outs_in, sums, final_in,
    ld_s, own_s, kv_s, kv_r, w_s, w_r, p_s, p_r, t_s, t_r, o_s, o_r, f_s, f_r,
):
    rows, heads, width = q_raw.shape
    half = rows // 2
    piece = half // 2
    depth, cols = wup.shape[1], wup.shape[2]
    model = ow.shape[1]
    pair = 2 * depth
    sp, core = lax.axis_index("sp"), lax.axis_index("tp")
    x, y, z = sp % 2, (sp // 2) % 2, sp // 4
    zh = z // 2
    zmate = z + 1 - 2 * (z % 2)
    far = [2 - zh, 3 * (1 - zh)]
    zs = [z, zmate] + far
    zc = [2 * zh, 2 * zh + 1] + far

    def at(dx, dy, zz):
        return (zz * 2 + (y + dy) % 2) * 2 + (x + dx) % 2

    def rank(dx, zz):
        return zz % 2 * 2 + (x + dx) % 2

    sent = []

    def send(src, dst, ss, rs, spi, tpi):
        c = pltpu.make_async_remote_copy(
            src_ref=src, dst_ref=dst, send_sem=ss, recv_sem=rs,
            device_id=(spi, tpi), device_id_type=MESH,
        )
        c.start()
        sent.append(c)

    def arrive(dst, ss, rs):
        pltpu.make_async_remote_copy(
            src_ref=dst, dst_ref=dst, send_sem=ss, recv_sem=rs,
            device_id=(sp, 1 - core), device_id_type=MESH,
        ).wait_recv()

    loads = {}
    for i, (name, src, dst) in enumerate([
        ("k", k_hbm, k_raw), ("v", v_hbm, v_raw), ("doc", doc_hbm, doc_v), ("kg", kg_hbm, kg),
        ("cr", cr_hbm, cr), ("cc", cc_hbm, cc), ("sr", sr_hbm, sr), ("sc", sc_hbm, sc),
        ("q", q_hbm, q_raw), ("qg", qg_hbm, qg), ("ow", ow_hbm, ow), ("res", res_hbm, res),
        ("ng", ng_hbm, ng),
    ]):
        loads[name] = pltpu.make_async_copy(src, dst, ld_s.at[i])
        loads[name].start()
    weights = ((up_hbm, wup), (down_hbm, wdown))

    def columns(w, dx, zz):
        return weights[w][0].at[:, pl.ds(pl.multiple_of(rank(dx, zz) * cols, 128), cols)]

    own = []
    for w in (0, 1):
        own.append(pltpu.make_async_copy(columns(w, 0, z), weights[w][1].at[sp], own_s.at[w]))
        own[w].start()

    barrier = pltpu.get_barrier_semaphore()
    peers = [(at(dx, 0, zs[k]), core) for dx in (0, 1) for k in range(4) if dx or k]
    peers += [(at(0, 1, z), core), (sp, 1 - core)]
    for p in peers:
        pl.semaphore_signal(barrier, inc=1, device_id=p, device_id_type=MESH)

    def wait_loads(*names):
        for name in names:
            loads[name].wait()

    wait_loads("k", "v", "doc", "kg", "cr", "cc", "sr", "sc")
    grid_rows = rows // GRID

    def table(row, col):
        lines = row[pl.ds(sp * grid_rows, grid_rows)]
        return (lines[:, None, :] + col[...][None]).reshape(rows, width)

    cosine, sine = table(cr, cc), table(sr, sc)
    first = lax.broadcasted_iota(jnp.int32, (rows, width), 1) % (width // 2) < width // 4

    def norm_rope(v, gain):
        v = v * lax.rsqrt(jnp.mean(v * v, axis=-1, keepdims=True) + EPS) * gain[...]
        turned = jnp.where(
            first, pltpu.roll(v, width - width // 4, 1), pltpu.roll(v, width // 4, 1)
        )
        return (v * cosine + turned * sine).astype(BF16)

    def own_head(ref):
        both = ref[...].astype(F32)
        return jnp.where(core == 0, both[:, 0, :], both[:, 1, :])

    kv_all[sp, 0:rows] = norm_rope(own_head(k_raw), kg)
    kv_all[sp, rows : 2 * rows] = own_head(v_raw).astype(BF16)
    docs = doc_v[...].astype(F32)
    lines = [docs[:, i * width : (i + 1) * width] for i in range(rows // width)]
    pad = kv_all.shape[1] - 2 * rows - len(lines)
    lines.append(jnp.zeros((pad, width), F32))
    kv_all[sp, 2 * rows :] = jnp.concatenate(lines, axis=0).astype(BF16)

    pl.semaphore_wait(barrier, len(peers))

    def send_kv(i, slot, spi):
        send(kv_all.at[slot], kv_all.at[slot], kv_s.at[i], kv_r.at[slot], spi, core)

    def wait_kv(slot):
        arrive(kv_all.at[slot], kv_s.at[0], kv_r.at[slot])

    def send_weight(w, dx, k):
        target = at(dx, 0, zs[k])
        send(
            columns(w, dx, zs[k]), weights[w][1].at[sp],
            w_s.at[w, dx * 4 + k], w_r.at[w, sp], target, core,
        )

    def wait_weight(w, dx, dy, zz):
        i = at(dx, dy, zz)
        arrive(weights[w][1].at[i], w_s.at[w, 0], w_r.at[w, i])

    def forward_weight(w, dx, k):
        i = at(dx, 0, zs[k])
        dst = weights[w][1]
        if dx or k:
            wait_weight(w, dx, 0, zs[k])
            src = dst.at[i]
        else:
            src = columns(w, 0, z)
        send(src, dst.at[i], w_s.at[w, 8 + dx * 4 + k], w_r.at[w, i], at(0, 1, z), core)

    for k in (1, 2, 3):
        send_kv(k, sp, at(0, 0, zs[k]))
    send_kv(0, sp, at(1, 0, z))
    send_kv(4, sp, at(0, 1, z))
    for k in (1, 2, 3):
        send_weight(0, 0, k)

    wait_loads("q", "qg")
    wide = q_raw[...].astype(F32)
    for h in range(heads):
        q_rot[h] = norm_rope(wide[:, h, :], qg)
    dcol[...] = jnp.broadcast_to(docs, (width, rows)).T

    for k in (1, 2, 3):
        i = at(0, 0, zs[k])
        wait_kv(i)
        send_kv(4 + k, i, at(1, 0, z))
        send_kv(8 + k, i, at(0, 1, z))

    for h in range(heads):
        lines = pl.ds(h * rows, rows)
        peak_s[lines] = jnp.full((rows, width), NEG, F32)
        den_s[lines] = jnp.zeros((rows, width), F32)
        acc_s[lines] = jnp.zeros((rows, width), F32)
    scale = float(width ** (-0.5) * np.log2(np.e))
    tiles = rows // width

    def attend(slots):
        for b, i in enumerate(slots):
            theirs = kv_all[i, 2 * rows :].astype(F32)
            for t in range(tiles):
                bias[:, (b * tiles + t) * width : (b * tiles + t + 1) * width] = jnp.where(
                    dcol[...] == theirs[t : t + 1], 0.0, NEG
                )
        for h in range(heads):
            lines = pl.ds(h * rows, rows)
            scores = []
            for b, i in enumerate(slots):
                s = lax.dot_general(
                    q_rot[h], kv_all[i, 0:rows], NT, preferred_element_type=F32
                )
                scores.append(s * scale + bias[:, b * rows : (b + 1) * rows])
            top = functools.reduce(
                jnp.maximum,
                [s[:, t * width : (t + 1) * width] for s in scores for t in range(tiles)],
            )
            peak = peak_s[lines]
            new_peak = jnp.maximum(peak, jnp.max(top, axis=-1, keepdims=True))
            peak_s[lines] = new_peak
            decay = jnp.exp2(peak - new_peak)
            spread = jnp.concatenate([new_peak] * tiles, axis=1)
            probs = [jnp.exp2(s - spread) for s in scores]
            den_s[lines] = den_s[lines] * decay + functools.reduce(
                jnp.add,
                [p[:, t * width : (t + 1) * width] for p in probs for t in range(tiles)],
            )
            acc_s[lines] = acc_s[lines] * decay + functools.reduce(
                jnp.add,
                [
                    jnp.dot(p.astype(BF16), kv_all[i, rows : 2 * rows], preferred_element_type=F32)
                    for i, p in zip(slots, probs)
                ],
            )

    def column(dx, dy):
        return [at(dx, dy, zz) for zz in zs]

    attend(column(0, 0))
    for k in (0, 1):
        i = at(1, 0, zs[k])
        wait_kv(i)
        send_kv(12 + k, i, at(0, 1, z))
    for k in (0, 1):
        wait_kv(at(0, 1, zs[k]))
    for k in (2, 3):
        i = at(0, 1, zs[k])
        wait_kv(i)
        send_kv(12 + k, i, at(1, 0, z))
    for k in (2, 3):
        wait_kv(at(1, 0, zs[k]))
    for k in (0, 1, 2, 3):
        send_weight(0, 1, k)
    forward_weight(0, 0, 0)
    attend(column(1, 0))
    attend(column(0, 1))
    forward_weight(0, 0, 1)
    for k in range(4):
        wait_kv(at(1, 1, zs[k]))
    attend(column(1, 1))
    forward_weight(0, 1, 0)
    for h in range(heads):
        lines = pl.ds(h * rows, rows)
        denom = jnp.sum(den_s[lines], axis=-1, keepdims=True)
        attn[:, h * width : (h + 1) * width] = (acc_s[lines] / denom).astype(BF16)

    tile = 256
    wait_loads("ow", "res", "ng")

    def project(owner, p, dst):
        mine = pl.ds(pl.multiple_of(owner * half + p * piece, piece), piece)

        @pl.loop(0, model // (2 * tile))
        def _(t):
            lanes = pl.ds(pl.multiple_of(t * 2 * tile, 2 * tile), 2 * tile)
            dst[p, :, lanes] = jnp.dot(
                attn[mine], ow[:, lanes], preferred_element_type=F32
            ).astype(BF16)

    for p in (0, 1):
        project(1 - core, p, part)
        send(part.at[p], part_in.at[p], p_s.at[p], p_r.at[p], sp, 1 - core)
    for p in (0, 1):
        project(core, p, own_part)
    group = 32
    xm, zm = at(1, 0, z), at(0, 0, zmate)
    n_tok = [0]

    def send_tok(src, dst, p, spi, tpi):
        i = n_tok[0]
        n_tok[0] += 1
        rc, c = dst
        send(tok.at[src[0], src[1], p], tok.at[rc, c, p], t_s.at[i], t_r.at[rc, c, p], spi, tpi)

    def wait_tok(rc, c, p):
        arrive(tok.at[rc, c, p], t_s.at[0], t_r.at[rc, c, p])

    for p in (0, 1):
        arrive(part_in.at[p], p_s.at[p], p_r.at[p])

        @pl.loop(0, piece // group)
        def _(t):
            rws = pl.ds(pl.multiple_of(t * group, group), group)
            branch = own_part[p, rws].astype(F32) + part_in[p, rws].astype(F32)
            rres = pl.ds(pl.multiple_of(core * half + p * piece + t * group, group), group)
            m = (res[rres].astype(F32) + branch).astype(BF16)
            mid[pl.ds(pl.multiple_of(p * piece + t * group, group), group)] = m
            full = m.astype(F32)
            inv = lax.rsqrt(jnp.mean(full * full, axis=-1, keepdims=True) + EPS)
            tok[0, 0, p, rws] = (full * inv * ng[...]).astype(BF16)

        if p == 0:
            send_tok((0, 0), (1, 0), 0, xm, core)
            send_tok((0, 0), (0, 1), 0, sp, 1 - core)
        else:
            send_tok((0, 0), (2, 0), 1, zm, core)
            send_tok((0, 0), (0, 1), 1, sp, 1 - core)
    send_tok((0, 0), (2, 0), 0, zm, core)
    send_tok((0, 0), (1, 0), 1, xm, core)
    forward_weight(0, 1, 1)
    wait_tok(1, 0, 0)
    send_tok((1, 0), (3, 0), 0, zm, core)
    send_tok((1, 0), (1, 1), 0, sp, 1 - core)
    wait_tok(2, 0, 1)
    send_tok((2, 0), (3, 0), 1, xm, core)
    send_tok((2, 0), (2, 1), 1, sp, 1 - core)
    for k in (1, 2, 3):
        send_weight(1, 0, k)
    for k in (0, 1, 2, 3):
        send_weight(1, 1, k)
    for k in (2, 3):
        for dx in (0, 1):
            forward_weight(0, dx, k)
    forward_weight(1, 0, 0)
    own[0].wait()
    wait_tok(1, 0, 1)
    send_tok((1, 0), (1, 1), 1, sp, 1 - core)
    wait_tok(2, 0, 0)
    send_tok((2, 0), (2, 1), 0, sp, 1 - core)
    for p in (0, 1):
        wait_tok(3, 0, p)
        send_tok((3, 0), (3, 1), p, sp, 1 - core)

    def raise_part(rc, dy, last):
        @pl.loop(0, cols // tile)
        def _(t):
            lanes = pl.ds(pl.multiple_of(t * tile, tile), tile)
            total = None
            for zz in range(4):
                block = (zz * 2 + (y + dy) % 2) * 2
                feats = pl.ds(pl.multiple_of(block * depth, pair), pair)
                tokens = tok[rc, :, :, :, feats].reshape(rows, pair)
                w = wup[pl.ds(block, 2), :, lanes].reshape(pair, tile)
                term = jnp.dot(tokens, w, preferred_element_type=F32)
                total = term if total is None else total + term
            if last:
                total = racc[rc, :, lanes] + total
                hidden[rc, :, lanes] = jnp.square(jnp.maximum(total, 0.0)).astype(BF16)
            else:
                racc[rc, :, lanes] = total

    for rc in range(4):
        for p in (0, 1):
            wait_tok(rc, 1, p)
        raise_part(rc, 0, False)
    for k in range(4):
        for dx in (0, 1):
            wait_weight(0, dx, 1, zs[k])
    for rc in range(4):
        raise_part(rc, 1, True)

    own[1].wait()

    def lower(j, dy, zz):
        block = (zz * 2 + (y + dy) % 2) * 2
        w = wdown[pl.ds(block, 2)].reshape(pair, cols)
        for rc in range(4):
            o = lax.dot_general(hidden[rc], w, NT, preferred_element_type=F32).astype(BF16)
            outs[j, 0, rc] = o[:half]
            outs[j, 1, rc] = o[half:]
        send(outs.at[j, 1], outs_in.at[j], o_s.at[j], o_r.at[j], sp, 1 - core)

    mates = (None, xm, zm, at(1, 0, zmate))

    def combine(j):
        arrive(outs_in.at[j], o_s.at[j], o_r.at[j])
        for rc in (3, 1, 2):
            sums[j, rc - 1] = (
                outs[j, 0, rc].astype(F32) + outs_in[j, rc].astype(F32)
            ).astype(BF16)
            send(
                sums.at[j, rc - 1], final_in.at[j, rc - 1],
                f_s.at[j, rc - 1], f_r.at[j, rc - 1], mates[rc], core,
            )

    def finish(j, dy, zz):
        block = (zz * 2 + (y + dy) % 2) * 2
        total = outs[j, 0, 0].astype(F32) + outs_in[j, 0].astype(F32)
        for rc in (1, 2, 3):
            arrive(final_in.at[j, rc - 1], f_s.at[j, rc - 1], f_r.at[j, rc - 1])
            total += final_in[j, rc - 1].astype(F32)
        lanes = pl.ds(pl.multiple_of(block * depth, pair), pair)
        out_ref[:, lanes] = (mid[:, lanes].astype(F32) + total).astype(BF16)

    order = [(0, 0), (0, 1), (1, 0), (1, 1), (0, 2), (1, 2), (0, 3), (1, 3)]
    for j, (dy, k) in enumerate(order):
        if dy == 0:
            if k == 0:
                for dx, kk in ((1, 0), (0, 1), (1, 1)):
                    forward_weight(1, dx, kk)
            elif k > 1:
                for dx in (0, 1):
                    forward_weight(1, dx, k)
        else:
            for dx in (0, 1):
                wait_weight(1, dx, 1, zc[k])
        lower(j, dy, zc[k])
        combine(j)
        if j >= 3:
            finish(j - 3, order[j - 3][0], zc[order[j - 3][1]])
    for j in range(5, 8):
        finish(j, order[j][0], zc[order[j][1]])

    for c in sent:
        c.wait_send()


def fused_body(
    queries, keys, values, documents, query_gain, key_gain, out_weight, residual, norm_gain,
    up_weight, down_weight,
):
    rows, heads, width = queries.shape
    n_sp = lax.axis_size("sp")
    model = residual.shape[1]
    depth, cols = up_weight.shape[0], up_weight.shape[1] // 4
    half = rows // 2
    piece = half // 2
    pair = 2 * depth
    chunks = model // pair
    dma = pltpu.SemaphoreType.DMA
    vmem = pltpu.VMEM
    tables = rope_tables(n_sp * rows // GRID, width)
    operands = (
        queries, keys, values, documents[None, :], query_gain[None, :], key_gain[None, :],
        out_weight, residual, norm_gain[None, :], up_weight, down_weight, *tables,
    )
    loaded = [a for i, a in enumerate(operands) if i not in (9, 10)]
    return pl.pallas_call(
        layer_kernel,
        out_shape=jax.ShapeDtypeStruct((half, model), BF16),
        in_specs=[pl.BlockSpec(memory_space=pl.ANY)] * len(operands),
        out_specs=pl.BlockSpec(memory_space=pltpu.VMEM),
        scratch_shapes=[vmem(a.shape, a.dtype) for a in loaded] + [
            vmem((heads, rows, width), BF16),
            vmem((n_sp, 2 * rows + 16, width), BF16),
            vmem((rows, width), F32),
            vmem((rows, 4 * rows), F32),
            vmem((heads * rows, width), F32),
            vmem((heads * rows, width), F32),
            vmem((heads * rows, width), F32),
            vmem((rows, heads * width), BF16),
            vmem((n_sp, depth, cols), BF16),
            vmem((n_sp, depth, cols), BF16),
            vmem((2, piece, model), BF16),
            vmem((2, piece, model), BF16),
            vmem((2, piece, model), BF16),
            vmem((half, model), BF16),
            vmem((4, 2, 2, piece, model), BF16),
            vmem((4, rows, cols), F32),
            vmem((4, rows, cols), BF16),
            vmem((chunks, 2, 4, half, pair), BF16),
            vmem((chunks, 4, half, pair), BF16),
            vmem((chunks, 3, half, pair), BF16),
            vmem((chunks, 3, half, pair), BF16),
            dma((13,)), dma((2,)), dma((16,)), dma((n_sp,)), dma((2, 16)), dma((2, n_sp)),
            dma((2,)), dma((2,)), dma((16,)), dma((4, 2, 2)), dma((chunks,)), dma((chunks,)),
            dma((chunks, 3)), dma((chunks, 3)),
        ],
        compiler_params=pltpu.CompilerParams(
            collective_id=0, has_side_effects=True, vmem_limit_bytes=60 * 1024 * 1024
        ),
    )(*operands)


def solution(mesh):
    in_specs = (
        P("sp", "tp", None),
        P("sp", None, None),
        P("sp", None, None),
        P("sp"),
        P(),
        P(),
        P("tp", None),
        P("sp", None),
        P(),
        P("sp", "tp"),
        P("sp", "tp"),
    )
    out_specs = P(("sp", "tp"), None)
    fused = mesh.shape["tp"] == 2 and mesh.shape["sp"] == 16
    return jax.shard_map(fused_body if fused else body, mesh=mesh, in_specs=in_specs, out_specs=out_specs, check_vma=False)
```

time: 181 us -> 130 us (0.72)
  Pallas kernels: 171 us -> 128 us
  other arithmetic: 5.26 us -> 0 us
  local copies, waits for them, and re-layouts: 3.97 us -> 1.88 us
    pallas_call x1, Pallas kernels: 171 us -> 128 us  [fused_body(): pl.pallas_call(layer_kernel, out_shape=jax.ShapeDtypeStruct((half, model)...]
where the time goes in v1:
time: 130 us
  Pallas kernels  128 us (98%)
  local copies, waits for them, and re-layouts  1.88 us (1%)
    pallas_call x1, Pallas kernels, fused_body(): pl.pallas_call(layer_kernel, out_shape=jax.ShapeDtypeStruct((half, model)...  128 us

profile of v1, /device:TPU:0, one launch (start us, length us, event | category | flops | bytes accessed | tf_op | source)
XLA Modules:
  0.0 129.8 jit_solution(3182358289794180398)
XLA Ops:
  0.0 127.9 %shard_map.145 = bf16[128,2048]{1,0:T(8,128)(2,1)} custom-call(bf16[256,4,128]{2,1,0:T(4,128)(2,1)} %q_hbm.1, bf16[256,2,128]{2,1,0:T(2,128)(2,1)} %k_hbm.1, bf16[256,2,128]{2,1,0:T(2,128)(2,1)} %v_hbm.1, s32[1,256]{1,0:T(1,128)} %bitcast.5, f32[1,128]{1,0:T(1,128)} %bitcast.6, f32[1,128]{1,0:T(1,128)} %bitcast.7, bf16[512,2048]{1,0:T(8,128)(2,1)} %ow_hbm.1, ...), custom_call_target="tpu_custom_call" | custom-call | tf_op jit(solution)/shard_map/pallas_call | solution.py:573
  127.9 1.9 %copy.17 = bf16[128,2048]{1,0:T(8,128)(2,1)} copy(bf16[128,2048]{1,0:T(8,128)(2,1)} %shard_map.145) | data formatting | bytes 1048576

commit v2 on v1

--- a/solution.py
+++ b/solution.py
@@ -145,6 +145,20 @@
 
 
 NEG = -1e30
+CHUNKS = ((0, 0), (0, 1), (1, 0), (0, 2), (1, 1), (0, 3), (1, 2), (1, 3))
+STRAIGHT = 0
+SCHEDULE = (
+    "K1", "K2", "K3", "n001", "n002", "n003", "A0", "R0", "R1", "A1",
+    "A2", "y000", "n010", "n011", "A3", "y001", "P0", "y010", "M0", "x0",
+    "M1", "z1", "z0", "x1", "n012", "n013", "n110", "n101", "n111", "m102",
+    "m112", "m103", "m113", "y011", "r10", "r21", "e102", "e112", "e103", "e113",
+    "y002", "y003", "y100", "y012", "y013", "U0", "r11", "r20", "U1", "U2",
+    "y110", "y101", "y111", "r30", "r31", "U3", "V0", "L0", "C0", "L1",
+    "C1", "y102", "y112", "L2", "C2", "Z0", "L3", "C3", "Z1", "y103",
+    "y113", "L4", "C4", "Z2", "F0", "L5", "C5", "Z3", "F1", "L6",
+    "C6", "Z4", "F2", "L7", "C7", "Z5", "Z6", "Z7", "F3", "F4",
+    "F5", "F6", "F7",
+)
 
 
 def rope_tables(n_rows, width):
@@ -193,12 +207,25 @@
 
     sent = []
 
-    def send(src, dst, ss, rs, spi, tpi):
+    inner = (z == 1) | (z == 2)
+    n_sp = kv_all.shape[0]
+    reach = n_sp // 2 + 1
+    low = n_sp // 4 - 1
+    lone = (sp == low) | (sp == low + reach)
+    across = jnp.where(sp == low, low + reach, low)
+    sometimes = []
+
+    def send(src, dst, ss, rs, spi, tpi, start=True, cond=None):
         c = pltpu.make_async_remote_copy(
             src_ref=src, dst_ref=dst, send_sem=ss, recv_sem=rs,
             device_id=(spi, tpi), device_id_type=MESH,
         )
-        c.start()
+        if cond is not None:
+            pl.when(cond)(c.start)
+            sometimes.append((cond, c))
+            return
+        if start:
+            c.start()
         sent.append(c)
 
     def arrive(dst, ss, rs):
@@ -227,10 +254,12 @@
         own[w].start()
 
     barrier = pltpu.get_barrier_semaphore()
-    peers = [(at(dx, 0, zs[k]), core) for dx in (0, 1) for k in range(4) if dx or k]
-    peers += [(at(0, 1, z), core), (sp, 1 - core)]
+    peers = [(at(0, 0, zz), core) for zz in zs[1:]]
+    peers += [(at(1, 0, z), core), (at(1, 0, zmate), core), (at(0, 1, z), core), (sp, 1 - core)]
+    peers += [(at(1, 1, 3 - z), core)]
     for p in peers:
         pl.semaphore_signal(barrier, inc=1, device_id=p, device_id_type=MESH)
+
 
     def wait_loads(*names):
         for name in names:
@@ -265,53 +294,65 @@
     lines.append(jnp.zeros((pad, width), F32))
     kv_all[sp, 2 * rows :] = jnp.concatenate(lines, axis=0).astype(BF16)
 
+    for dx, dy in ((0, 0), (1, 0), (0, 1), (1, 1)):
+        empty = at(dx, dy, zs[3])
+
+        @pl.when(jnp.logical_not(inner | (lone & (empty == across))))
+        def _():
+            kv_all[empty] = jnp.full(kv_all.shape[1:], -1.0, BF16)
+
     pl.semaphore_wait(barrier, len(peers))
 
-    def send_kv(i, slot, spi):
-        send(kv_all.at[slot], kv_all.at[slot], kv_s.at[i], kv_r.at[slot], spi, core)
-
-    def wait_kv(slot):
+
+    def send_kv(i, slot, spi, cond=None):
+        send(
+            kv_all.at[slot], kv_all.at[slot], kv_s.at[i], kv_r.at[slot], spi, core, cond=cond
+        )
+
+    def only(k):
+        return inner if k == 3 else None
+
+    def wait_kv(slot, cond=None):
+        if cond is not None:
+            pl.when(cond)(lambda: wait_kv(slot))
+            return
         arrive(kv_all.at[slot], kv_s.at[0], kv_r.at[slot])
 
-    def send_weight(w, dx, k):
-        target = at(dx, 0, zs[k])
+    def send_weight(w, dx, k, start=True):
         send(
             columns(w, dx, zs[k]), weights[w][1].at[sp],
-            w_s.at[w, dx * 4 + k], w_r.at[w, sp], target, core,
+            w_s.at[w, dx * 4 + k], w_r.at[w, sp], at(dx, 0, zs[k]), core, start,
         )
+
+    def send_weight_if(cond, w, dx, k):
+        count = len(sent)
+        pl.when(cond)(lambda: send_weight(w, dx, k))
+        del sent[count:]
 
     def wait_weight(w, dx, dy, zz):
         i = at(dx, dy, zz)
         arrive(weights[w][1].at[i], w_s.at[w, 0], w_r.at[w, i])
 
-    def forward_weight(w, dx, k):
+    def pass_weight(w, dx, k, across):
         i = at(dx, 0, zs[k])
         dst = weights[w][1]
-        if dx or k:
-            wait_weight(w, dx, 0, zs[k])
-            src = dst.at[i]
-        else:
-            src = columns(w, 0, z)
-        send(src, dst.at[i], w_s.at[w, 8 + dx * 4 + k], w_r.at[w, i], at(0, 1, z), core)
+        src = dst.at[i] if dx or k else columns(w, 0, z)
+        send(
+            src, dst.at[i], w_s.at[w, (16 if across else 8) + dx * 4 + k], w_r.at[w, i],
+            at(0, 0, (z + 2) % 4) if across else at(0, 1, z), core,
+        )
 
     for k in (1, 2, 3):
-        send_kv(k, sp, at(0, 0, zs[k]))
+        send_kv(k, sp, at(0, 0, zs[k]), only(k))
     send_kv(0, sp, at(1, 0, z))
     send_kv(4, sp, at(0, 1, z))
-    for k in (1, 2, 3):
-        send_weight(0, 0, k)
+    send_kv(16, sp, across, lone)
 
     wait_loads("q", "qg")
     wide = q_raw[...].astype(F32)
     for h in range(heads):
         q_rot[h] = norm_rope(wide[:, h, :], qg)
     dcol[...] = jnp.broadcast_to(docs, (width, rows)).T
-
-    for k in (1, 2, 3):
-        i = at(0, 0, zs[k])
-        wait_kv(i)
-        send_kv(4 + k, i, at(1, 0, z))
-        send_kv(8 + k, i, at(0, 1, z))
 
     for h in range(heads):
         lines = pl.ds(h * rows, rows)
@@ -361,52 +402,57 @@
     def column(dx, dy):
         return [at(dx, dy, zz) for zz in zs]
 
-    attend(column(0, 0))
-    for k in (0, 1):
-        i = at(1, 0, zs[k])
-        wait_kv(i)
-        send_kv(12 + k, i, at(0, 1, z))
-    for k in (0, 1):
-        wait_kv(at(0, 1, zs[k]))
-    for k in (2, 3):
-        i = at(0, 1, zs[k])
-        wait_kv(i)
-        send_kv(12 + k, i, at(1, 0, z))
-    for k in (2, 3):
-        wait_kv(at(1, 0, zs[k]))
-    for k in (0, 1, 2, 3):
-        send_weight(0, 1, k)
-    forward_weight(0, 0, 0)
-    attend(column(1, 0))
-    attend(column(0, 1))
-    forward_weight(0, 0, 1)
-    for k in range(4):
-        wait_kv(at(1, 1, zs[k]))
-    attend(column(1, 1))
-    forward_weight(0, 1, 0)
-    for h in range(heads):
-        lines = pl.ds(h * rows, rows)
-        denom = jnp.sum(den_s[lines], axis=-1, keepdims=True)
-        attn[:, h * width : (h + 1) * width] = (acc_s[lines] / denom).astype(BF16)
+    def relay_z(k):
+        i = at(0, 0, zs[k])
+        wait_kv(i, only(k))
+        send_kv(4 + k, i, at(1, 0, z), only(k))
+        send_kv(8 + k, i, at(0, 1, z), only(k))
+
+    def relay_y():
+        for k in (0, 1):
+            i = at(1, 0, zs[k])
+            wait_kv(i)
+            send_kv(12 + k, i, at(0, 1, z))
+
+    def relay_x():
+        for k in (2, 3):
+            i = at(0, 1, zs[k])
+            wait_kv(i, only(k))
+            send_kv(12 + k, i, at(1, 0, z), only(k))
+
+    def attend_column(dx, dy, ks):
+        for k in ks:
+            wait_kv(at(dx, dy, zs[k]), only(k))
+        if dx and dy:
+            wait_kv(across, lone)
+        attend(column(dx, dy))
+
+    def attention_out():
+        for h in range(heads):
+            lines = pl.ds(h * rows, rows)
+            denom = jnp.sum(den_s[lines], axis=-1, keepdims=True)
+            attn[:, h * width : (h + 1) * width] = (acc_s[lines] / denom).astype(BF16)
 
     tile = 256
-    wait_loads("ow", "res", "ng")
-
-    def project(owner, p, dst):
-        mine = pl.ds(pl.multiple_of(owner * half + p * piece, piece), piece)
-
-        @pl.loop(0, model // (2 * tile))
+
+    def project(owner, dst):
+        mine = pl.ds(pl.multiple_of(owner * half, half), half)
+        wide = 4 * tile
+
+        @pl.loop(0, model // wide)
         def _(t):
-            lanes = pl.ds(pl.multiple_of(t * 2 * tile, 2 * tile), 2 * tile)
-            dst[p, :, lanes] = jnp.dot(
-                attn[mine], ow[:, lanes], preferred_element_type=F32
-            ).astype(BF16)
-
-    for p in (0, 1):
-        project(1 - core, p, part)
-        send(part.at[p], part_in.at[p], p_s.at[p], p_r.at[p], sp, 1 - core)
-    for p in (0, 1):
-        project(core, p, own_part)
+            lanes = pl.ds(pl.multiple_of(t * wide, wide), wide)
+            o = jnp.dot(attn[mine], ow[:, lanes], preferred_element_type=F32).astype(BF16)
+            dst[0, :, lanes] = o[:piece]
+            dst[1, :, lanes] = o[piece:]
+
+    def project_all():
+        wait_loads("ow", "res", "ng")
+        project(1 - core, part)
+        for p in (0, 1):
+            send(part.at[p], part_in.at[p], p_s.at[p], p_r.at[p], sp, 1 - core)
+        project(core, own_part)
+
     group = 32
     xm, zm = at(1, 0, z), at(0, 0, zmate)
     n_tok = [0]
@@ -417,10 +463,13 @@
         rc, c = dst
         send(tok.at[src[0], src[1], p], tok.at[rc, c, p], t_s.at[i], t_r.at[rc, c, p], spi, tpi)
 
+    def to_partner(rc, p):
+        send_tok((rc, 0), (rc, 1), p, sp, 1 - core)
+
     def wait_tok(rc, c, p):
         arrive(tok.at[rc, c, p], t_s.at[0], t_r.at[rc, c, p])
 
-    for p in (0, 1):
+    def middle(p):
         arrive(part_in.at[p], p_s.at[p], p_r.at[p])
 
         @pl.loop(0, piece // group)
@@ -434,69 +483,64 @@
             inv = lax.rsqrt(jnp.mean(full * full, axis=-1, keepdims=True) + EPS)
             tok[0, 0, p, rws] = (full * inv * ng[...]).astype(BF16)
 
-        if p == 0:
-            send_tok((0, 0), (1, 0), 0, xm, core)
-            send_tok((0, 0), (0, 1), 0, sp, 1 - core)
-        else:
-            send_tok((0, 0), (2, 0), 1, zm, core)
-            send_tok((0, 0), (0, 1), 1, sp, 1 - core)
-    send_tok((0, 0), (2, 0), 0, zm, core)
-    send_tok((0, 0), (1, 0), 1, xm, core)
-    forward_weight(0, 1, 1)
-    wait_tok(1, 0, 0)
-    send_tok((1, 0), (3, 0), 0, zm, core)
-    send_tok((1, 0), (1, 1), 0, sp, 1 - core)
-    wait_tok(2, 0, 1)
-    send_tok((2, 0), (3, 0), 1, xm, core)
-    send_tok((2, 0), (2, 1), 1, sp, 1 - core)
-    for k in (1, 2, 3):
-        send_weight(1, 0, k)
-    for k in (0, 1, 2, 3):
-        send_weight(1, 1, k)
-    for k in (2, 3):
-        for dx in (0, 1):
-            forward_weight(0, dx, k)
-    forward_weight(1, 0, 0)
-    own[0].wait()
-    wait_tok(1, 0, 1)
-    send_tok((1, 0), (1, 1), 1, sp, 1 - core)
-    wait_tok(2, 0, 0)
-    send_tok((2, 0), (2, 1), 0, sp, 1 - core)
-    for p in (0, 1):
-        wait_tok(3, 0, p)
-        send_tok((3, 0), (3, 1), p, sp, 1 - core)
-
-    def raise_part(rc, dy, last):
+        to_partner(0, p)
+
+    def relay_tok(rc, p, spi):
+        wait_tok(rc, 0, p)
+        if spi is not None:
+            send_tok((rc, 0), (3, 0), p, spi, core)
+        to_partner(rc, p)
+
+    waited = set()
+
+    def wait_near(w, dx, k):
+        if (dx or k) and (w, dx, k) not in waited:
+            waited.add((w, dx, k))
+            wait_weight(w, dx, 0, zs[k])
+
+    def block_of(dy, zz):
+        block = (zz * 2 + (y + dy) % 2) * 2
+        return block, pl.ds(pl.multiple_of(block * depth, pair), pair)
+
+    def raise_first(rc):
+        if rc == 0:
+            own[0].wait()
+        for p in (0, 1):
+            wait_tok(rc, 1, p)
+        total = None
+        for zz in range(4):
+            block, feats = block_of(0, zz)
+            tokens = tok[rc, :, :, :, feats].reshape(rows, pair)
+            w = wup[pl.ds(block, 2)].reshape(pair, cols)
+            term = jnp.dot(tokens, w, preferred_element_type=F32)
+            total = term if total is None else total + term
+        racc[rc] = total
+
+    def raise_second():
+        for zz in zs:
+            for dx in (0, 1):
+                wait_weight(0, dx, 1, zz)
+
         @pl.loop(0, cols // tile)
         def _(t):
             lanes = pl.ds(pl.multiple_of(t * tile, tile), tile)
-            total = None
+            total = racc[:, :, lanes].reshape(4 * rows, tile)
             for zz in range(4):
-                block = (zz * 2 + (y + dy) % 2) * 2
-                feats = pl.ds(pl.multiple_of(block * depth, pair), pair)
-                tokens = tok[rc, :, :, :, feats].reshape(rows, pair)
+                block, feats = block_of(1, zz)
+                tokens = tok[:, :, :, :, feats].reshape(4 * rows, pair)
                 w = wup[pl.ds(block, 2), :, lanes].reshape(pair, tile)
-                term = jnp.dot(tokens, w, preferred_element_type=F32)
-                total = term if total is None else total + term
-            if last:
-                total = racc[rc, :, lanes] + total
-                hidden[rc, :, lanes] = jnp.square(jnp.maximum(total, 0.0)).astype(BF16)
-            else:
-                racc[rc, :, lanes] = total
-
-    for rc in range(4):
-        for p in (0, 1):
-            wait_tok(rc, 1, p)
-        raise_part(rc, 0, False)
-    for k in range(4):
-        for dx in (0, 1):
-            wait_weight(0, dx, 1, zs[k])
-    for rc in range(4):
-        raise_part(rc, 1, True)
-
-    own[1].wait()
-
-    def lower(j, dy, zz):
+                total = total + jnp.dot(tokens, w, preferred_element_type=F32)
+            raised = jnp.square(jnp.maximum(total, 0.0)).astype(BF16)
+            hidden[:, :, lanes] = raised.reshape(4, rows, tile)
+
+    def lower(j):
+        dy, k = CHUNKS[j]
+        zz = zc[k]
+        if dy:
+            for dx in (0, 1):
+                wait_weight(1, dx, 1, zz)
+        elif k == 0:
+            own[1].wait()
         block = (zz * 2 + (y + dy) % 2) * 2
         w = wdown[pl.ds(block, 2)].reshape(pair, cols)
         for rc in range(4):
@@ -505,49 +549,99 @@
             outs[j, 1, rc] = o[half:]
         send(outs.at[j, 1], outs_in.at[j], o_s.at[j], o_r.at[j], sp, 1 - core)
 
-    mates = (None, xm, zm, at(1, 0, zmate))
+    def merged(j, rc):
+        return outs[j, 0, rc].astype(F32) + outs_in[j, rc].astype(F32)
 
     def combine(j):
         arrive(outs_in.at[j], o_s.at[j], o_r.at[j])
-        for rc in (3, 1, 2):
-            sums[j, rc - 1] = (
-                outs[j, 0, rc].astype(F32) + outs_in[j, rc].astype(F32)
-            ).astype(BF16)
-            send(
-                sums.at[j, rc - 1], final_in.at[j, rc - 1],
-                f_s.at[j, rc - 1], f_r.at[j, rc - 1], mates[rc], core,
-            )
-
-    def finish(j, dy, zz):
+        for i, rc in ((0, 1), (1, 3)):
+            sums[j, i] = merged(j, rc).astype(BF16)
+        if j < STRAIGHT:
+            both = pl.ds(0, 2)
+            send(sums.at[j, both], final_in.at[j, both], f_s.at[j, 0], f_r.at[j, 0], xm, core)
+            return
+        sums[j, 2] = merged(j, 2).astype(BF16)
+        for i, mate in ((1, at(1, 0, zmate)), (0, xm), (2, zm)):
+            send(sums.at[j, i], final_in.at[j, i], f_s.at[j, i], f_r.at[j, i], mate, core)
+
+    def combine_z(j):
+        if j >= STRAIGHT:
+            return
+        both = pl.ds(0, 2)
+        arrive(final_in.at[j, both], f_s.at[j, 0], f_r.at[j, 0])
+        sums[j, 2] = (merged(j, 2) + final_in[j, 1].astype(F32)).astype(BF16)
+        send(sums.at[j, 2], final_in.at[j, 2], f_s.at[j, 2], f_r.at[j, 2], zm, core)
+
+    def finish(j):
+        dy, k = CHUNKS[j]
+        zz = zc[k]
         block = (zz * 2 + (y + dy) % 2) * 2
-        total = outs[j, 0, 0].astype(F32) + outs_in[j, 0].astype(F32)
-        for rc in (1, 2, 3):
-            arrive(final_in.at[j, rc - 1], f_s.at[j, rc - 1], f_r.at[j, rc - 1])
-            total += final_in[j, rc - 1].astype(F32)
+        total = merged(j, 0)
+        if j >= STRAIGHT:
+            for i in (0, 1):
+                arrive(final_in.at[j, i], f_s.at[j, i], f_r.at[j, i])
+                total += final_in[j, i].astype(F32)
+        else:
+            total += final_in[j, 0].astype(F32)
+        arrive(final_in.at[j, 2], f_s.at[j, 2], f_r.at[j, 2])
+        total += final_in[j, 2].astype(F32)
         lanes = pl.ds(pl.multiple_of(block * depth, pair), pair)
         out_ref[:, lanes] = (mid[:, lanes].astype(F32) + total).astype(BF16)
 
-    order = [(0, 0), (0, 1), (1, 0), (1, 1), (0, 2), (1, 2), (0, 3), (1, 3)]
-    for j, (dy, k) in enumerate(order):
-        if dy == 0:
-            if k == 0:
-                for dx, kk in ((1, 0), (0, 1), (1, 1)):
-                    forward_weight(1, dx, kk)
-            elif k > 1:
-                for dx in (0, 1):
-                    forward_weight(1, dx, k)
-        else:
-            for dx in (0, 1):
-                wait_weight(1, dx, 1, zc[k])
-        lower(j, dy, zc[k])
-        combine(j)
-        if j >= 3:
-            finish(j - 3, order[j - 3][0], zc[order[j - 3][1]])
-    for j in range(5, 8):
-        finish(j, order[j][0], zc[order[j][1]])
+    def step(op):
+        kind, code = op[0], [int(c) for c in op[1:]]
+        if kind == "n":
+            send_weight(*code)
+        elif kind == "m":
+            send_weight_if(inner, *code)
+            send_weight(*code, False)
+        elif kind == "e":
+            send_weight_if(jnp.logical_not(inner), *code)
+        elif kind == "f":
+            wait_near(*code)
+            pass_weight(*code, True)
+        elif kind == "y":
+            wait_near(*code)
+            pass_weight(*code, False)
+        elif kind == "K":
+            relay_z(code[0])
+        elif kind == "R":
+            (relay_x if code[0] else relay_y)()
+        elif kind == "A":
+            dx, dy = ((0, 0), (1, 0), (0, 1), (1, 1))[code[0]]
+            attend_column(dx, dy, ((), (2, 3), (0, 1), (0, 1, 2, 3))[code[0]])
+        elif kind == "P":
+            attention_out()
+            project_all()
+        elif kind == "M":
+            middle(code[0])
+        elif kind == "x":
+            send_tok((0, 0), (1, 0), code[0], xm, core)
+        elif kind == "z":
+            send_tok((0, 0), (2, 0), code[0], zm, core)
+        elif kind == "r":
+            rc, p = code
+            relay_tok(rc, p, zm if (rc, p) == (1, 0) else xm if (rc, p) == (2, 1) else None)
+        elif kind == "U":
+            raise_first(code[0])
+        elif kind == "V":
+            raise_second()
+        elif kind == "L":
+            lower(code[0])
+        elif kind == "C":
+            combine(code[0])
+        elif kind == "Z":
+            combine_z(code[0])
+        elif kind == "F":
+            finish(code[0])
+
+    for op in SCHEDULE:
+        step(op)
 
     for c in sent:
         c.wait_send()
+    for cond, c in sometimes:
+        pl.when(cond)(c.wait_send)
 
 
 def fused_body(
@@ -597,7 +691,7 @@
             vmem((chunks, 4, half, pair), BF16),
             vmem((chunks, 3, half, pair), BF16),
             vmem((chunks, 3, half, pair), BF16),
-            dma((13,)), dma((2,)), dma((16,)), dma((n_sp,)), dma((2, 16)), dma((2, n_sp)),
+            dma((13,)), dma((2,)), dma((17,)), dma((n_sp,)), dma((2, 24)), dma((2, n_sp)),
             dma((2,)), dma((2,)), dma((16,)), dma((4, 2, 2)), dma((chunks,)), dma((chunks,)),
             dma((chunks, 3)), dma((chunks, 3)),
         ],

time: 130 us -> 125 us (0.962)
  the two profiles are of different devices: /device:TPU:0 before, /device:TPU:20 now
where the time goes in v2:
time: 125 us
  Pallas kernels  123 us (98%)
  local copies, waits for them, and re-layouts  1.88 us (2%)
    pallas_call x1, Pallas kernels, fused_body(): pl.pallas_call(layer_kernel, out_shape=jax.ShapeDtypeStruct((half, model)...  123 us

profile of v2, /device:TPU:20, one launch (start us, length us, event | category | flops | bytes accessed | tf_op | source)
XLA Modules:
  0.0 124.9 jit_solution(10104315219074092336)
XLA Ops:
  0.0 123.0 %shard_map.145 = bf16[128,2048]{1,0:T(8,128)(2,1)} custom-call(bf16[256,4,128]{2,1,0:T(4,128)(2,1)} %q_hbm.1, bf16[256,2,128]{2,1,0:T(2,128)(2,1)} %k_hbm.1, bf16[256,2,128]{2,1,0:T(2,128)(2,1)} %v_hbm.1, s32[1,256]{1,0:T(1,128)} %bitcast.5, f32[1,128]{1,0:T(1,128)} %bitcast.6, f32[1,128]{1,0:T(1,128)} %bitcast.7, bf16[512,2048]{1,0:T(8,128)(2,1)} %ow_hbm.1, ...), custom_call_target="tpu_custom_call" | custom-call | tf_op jit(solution)/shard_map/pallas_call | solution.py:667
  123.0 1.9 %copy.17 = bf16[128,2048]{1,0:T(8,128)(2,1)} copy(bf16[128,2048]{1,0:T(8,128)(2,1)} %shard_map.145) | data formatting | bytes 1048576

commit v3 on v2

--- a/solution.py
+++ b/solution.py
@@ -149,10 +149,10 @@
 STRAIGHT = 0
 SCHEDULE = (
     "K1", "K2", "K3", "n001", "n002", "n003", "A0", "R0", "R1", "A1",
-    "A2", "y000", "n010", "n011", "A3", "y001", "P0", "y010", "M0", "x0",
-    "M1", "z1", "z0", "x1", "n012", "n013", "n110", "n101", "n111", "m102",
-    "m112", "m103", "m113", "y011", "r10", "r21", "e102", "e112", "e103", "e113",
-    "y002", "y003", "y100", "y012", "y013", "U0", "r11", "r20", "U1", "U2",
+    "A2", "y000", "n010", "n011", "n012", "n013", "A3", "y001", "P0", "M0",
+    "x0", "M1", "z1", "z0", "x1", "n110", "n101", "n111", "m102", "m112",
+    "m103", "m113", "y010", "y011", "r10", "r21", "e102", "e112", "e103", "e113",
+    "y002", "y012", "y003", "y013", "y100", "U0", "r11", "r20", "U1", "U2",
     "y110", "y101", "y111", "r30", "r31", "U3", "V0", "L0", "C0", "L1",
     "C1", "y102", "y112", "L2", "C2", "Z0", "L3", "C3", "Z1", "y103",
     "y113", "L4", "C4", "Z2", "F0", "L5", "C5", "Z3", "F1", "L6",
@@ -207,23 +207,11 @@
 
     sent = []
 
-    inner = (z == 1) | (z == 2)
-    n_sp = kv_all.shape[0]
-    reach = n_sp // 2 + 1
-    low = n_sp // 4 - 1
-    lone = (sp == low) | (sp == low + reach)
-    across = jnp.where(sp == low, low + reach, low)
-    sometimes = []
-
-    def send(src, dst, ss, rs, spi, tpi, start=True, cond=None):
+    def send(src, dst, ss, rs, spi, tpi, start=True):
         c = pltpu.make_async_remote_copy(
             src_ref=src, dst_ref=dst, send_sem=ss, recv_sem=rs,
             device_id=(spi, tpi), device_id_type=MESH,
         )
-        if cond is not None:
-            pl.when(cond)(c.start)
-            sometimes.append((cond, c))
-            return
         if start:
             c.start()
         sent.append(c)
@@ -256,10 +244,8 @@
     barrier = pltpu.get_barrier_semaphore()
     peers = [(at(0, 0, zz), core) for zz in zs[1:]]
     peers += [(at(1, 0, z), core), (at(1, 0, zmate), core), (at(0, 1, z), core), (sp, 1 - core)]
-    peers += [(at(1, 1, 3 - z), core)]
     for p in peers:
         pl.semaphore_signal(barrier, inc=1, device_id=p, device_id_type=MESH)
-
 
     def wait_loads(*names):
         for name in names:
@@ -294,28 +280,12 @@
     lines.append(jnp.zeros((pad, width), F32))
     kv_all[sp, 2 * rows :] = jnp.concatenate(lines, axis=0).astype(BF16)
 
-    for dx, dy in ((0, 0), (1, 0), (0, 1), (1, 1)):
-        empty = at(dx, dy, zs[3])
-
-        @pl.when(jnp.logical_not(inner | (lone & (empty == across))))
-        def _():
-            kv_all[empty] = jnp.full(kv_all.shape[1:], -1.0, BF16)
-
     pl.semaphore_wait(barrier, len(peers))
 
-
-    def send_kv(i, slot, spi, cond=None):
-        send(
-            kv_all.at[slot], kv_all.at[slot], kv_s.at[i], kv_r.at[slot], spi, core, cond=cond
-        )
-
-    def only(k):
-        return inner if k == 3 else None
-
-    def wait_kv(slot, cond=None):
-        if cond is not None:
-            pl.when(cond)(lambda: wait_kv(slot))
-            return
+    def send_kv(i, slot, spi):
+        send(kv_all.at[slot], kv_all.at[slot], kv_s.at[i], kv_r.at[slot], spi, core)
+
+    def wait_kv(slot):
         arrive(kv_all.at[slot], kv_s.at[0], kv_r.at[slot])
 
     def send_weight(w, dx, k, start=True):
@@ -343,10 +313,9 @@
         )
 
     for k in (1, 2, 3):
-        send_kv(k, sp, at(0, 0, zs[k]), only(k))
+        send_kv(k, sp, at(0, 0, zs[k]))
     send_kv(0, sp, at(1, 0, z))
     send_kv(4, sp, at(0, 1, z))
-    send_kv(16, sp, across, lone)
 
     wait_loads("q", "qg")
     wide = q_raw[...].astype(F32)
@@ -404,9 +373,9 @@
 
     def relay_z(k):
         i = at(0, 0, zs[k])
-        wait_kv(i, only(k))
-        send_kv(4 + k, i, at(1, 0, z), only(k))
-        send_kv(8 + k, i, at(0, 1, z), only(k))
+        wait_kv(i)
+        send_kv(4 + k, i, at(1, 0, z))
+        send_kv(8 + k, i, at(0, 1, z))
 
     def relay_y():
         for k in (0, 1):
@@ -417,14 +386,12 @@
     def relay_x():
         for k in (2, 3):
             i = at(0, 1, zs[k])
-            wait_kv(i, only(k))
-            send_kv(12 + k, i, at(1, 0, z), only(k))
+            wait_kv(i)
+            send_kv(12 + k, i, at(1, 0, z))
 
     def attend_column(dx, dy, ks):
         for k in ks:
-            wait_kv(at(dx, dy, zs[k]), only(k))
-        if dx and dy:
-            wait_kv(across, lone)
+            wait_kv(at(dx, dy, zs[k]))
         attend(column(dx, dy))
 
     def attention_out():
@@ -492,6 +459,7 @@
         to_partner(rc, p)
 
     waited = set()
+    inner = (z == 1) | (z == 2)
 
     def wait_near(w, dx, k):
         if (dx or k) and (w, dx, k) not in waited:
@@ -640,8 +608,6 @@
 
     for c in sent:
         c.wait_send()
-    for cond, c in sometimes:
-        pl.when(cond)(c.wait_send)
 
 
 def fused_body(
@@ -691,7 +657,7 @@
             vmem((chunks, 4, half, pair), BF16),
             vmem((chunks, 3, half, pair), BF16),
             vmem((chunks, 3, half, pair), BF16),
-            dma((13,)), dma((2,)), dma((17,)), dma((n_sp,)), dma((2, 24)), dma((2, n_sp)),
+            dma((13,)), dma((2,)), dma((16,)), dma((n_sp,)), dma((2, 24)), dma((2, n_sp)),
             dma((2,)), dma((2,)), dma((16,)), dma((4, 2, 2)), dma((chunks,)), dma((chunks,)),
             dma((chunks, 3)), dma((chunks, 3)),
         ],

time: 125 us -> 120 us (0.960)
  the two profiles are of different devices: /device:TPU:20 before, /device:TPU:0 now
where the time goes in v3:
time: 120 us
  Pallas kernels  118 us (98%)
  local copies, waits for them, and re-layouts  1.88 us (2%)
    pallas_call x1, Pallas kernels, fused_body(): pl.pallas_call(layer_kernel, out_shape=jax.ShapeDtypeStruct((half, model)...  118 us

profile of v3, /device:TPU:0, one launch (start us, length us, event | category | flops | bytes accessed | tf_op | source)
XLA Modules:
  0.0 119.8 jit_solution(3133151540706013979)
XLA Ops:
  0.0 117.9 %shard_map.145 = bf16[128,2048]{1,0:T(8,128)(2,1)} custom-call(bf16[256,4,128]{2,1,0:T(4,128)(2,1)} %q_hbm.1, bf16[256,2,128]{2,1,0:T(2,128)(2,1)} %k_hbm.1, bf16[256,2,128]{2,1,0:T(2,128)(2,1)} %v_hbm.1, s32[1,256]{1,0:T(1,128)} %bitcast.5, f32[1,128]{1,0:T(1,128)} %bitcast.6, f32[1,128]{1,0:T(1,128)} %bitcast.7, bf16[512,2048]{1,0:T(8,128)(2,1)} %ow_hbm.1, ...), custom_call_target="tpu_custom_call" | custom-call | tf_op jit(solution)/shard_map/pallas_call | solution.py:633
  118.0 1.9 %copy.17 = bf16[128,2048]{1,0:T(8,128)(2,1)} copy(bf16[128,2048]{1,0:T(8,128)(2,1)} %shard_map.145) | data formatting | bytes 1048576
